TPU v7x, 32 devices: a whole 2x2x4 slice. The times are simulated.
32 devices in a mesh: ep: 8 (over z, core), tp: 4 (over y, x).
Axes of the slice: x: 2, y: 2, z: 4, core: 2. Of those that a mesh axis runs over, the one named last changes fastest.
Arguments:
- tokens: bfloat16 [1024, 2048], P('ep', 'tp'), may hold values from -540 to 540
- expert_ids: int32 [1024, 2], P('ep'), may hold values from 0 to 7, all different within a row; in each aligned block of 128 rows (0 to 127, 128 to 255, ...) at most 64 rows name the same one
- gate_weights: float32 [1024, 2], P('ep'), may hold values from 0.1 to 1
- gain_in: float32 [2048], P('tp'), may hold values from 0.1 to 1.9
- gain_out: float32 [2048], P('tp'), may hold values from 0.1 to 1.9
- w_gate: bfloat16 [8, 2048, 8192], P('ep', None, 'tp'), may hold values from -0.125 to 0.125
- w_up: bfloat16 [8, 2048, 8192], P('ep', None, 'tp'), may hold values from -0.125 to 0.125
- w_down: bfloat16 [8, 8192, 2048], P('ep', 'tp'), may hold values from -0.397747564 to 0.397747564
Outputs:
- mixed: bfloat16 [1024, 2048], P('ep', 'tp')
Inputs may be any that keep to these rules, and one draw needn't show every extreme that they name: `expert_ids`: each row names 2 different experts. In the rows of one index of ep (aligned blocks of 128 rows) no expert is named by more than 64 rows, a bound that some block reaches.
All inputs are finite; a program needn't handle non-finite values.
Results may differ from a plain program's by a relative error of at most 0.018.
Values may be sent and summed in bfloat16 or wider, within the bound.
A program may use at most 64 MiB of HBM per device.

v0:
```python
import jax
import jax.numpy as jnp
from jax import lax
from jax.sharding import PartitionSpec as P

TOP = 2
NORM_EPS = 1e-06


def on_device(tokens, expert_ids, gate_weights, gain_in, gain_out, w_gate, w_up, w_down):
    count_tp = lax.axis_size("tp")
    count_ep = lax.axis_size("ep")
    tok_rows = tokens.shape[0]
    model_width = tokens.shape[1] * count_tp
    capacity = 2 * TOP * tok_rows // count_ep
    values = tokens.astype(jnp.float32)
    squares = lax.psum(jnp.sum(values * values, axis=1), "tp")
    normed = (values * lax.rsqrt(squares[:, None] / model_width + NORM_EPS) * gain_in).astype(
        jnp.bfloat16
    )
    flat_ids = expert_ids.reshape(-1)
    one_hot = (flat_ids[:, None] == jnp.arange(count_ep, dtype=jnp.int32)[None, :]).astype(
        jnp.int32
    )
    earlier = jnp.cumsum(one_hot, axis=0) - 1
    slot_index = jnp.sum(one_hot * earlier, axis=1)
    places = (flat_ids * capacity + slot_index).reshape(tok_rows, TOP)
    slot_rows = jnp.arange(count_ep * capacity, dtype=jnp.int32)
    picker = jnp.sum((slot_rows[:, None, None] == places[None, :, :]).astype(jnp.bfloat16), axis=2)
    gate_w = w_gate[0]
    up_w = w_up[0]
    down_w = w_down[0]
    outgoing = jnp.dot(picker, normed, preferred_element_type=jnp.float32).astype(jnp.bfloat16)
    arrived = lax.all_to_all(outgoing, "ep", split_axis=0, concat_axis=0, tiled=True)
    shard_part = lax.all_gather(arrived, "tp", axis=1, tiled=True)
    gate_part = jnp.dot(shard_part, gate_w, preferred_element_type=jnp.float32)
    up_part = jnp.dot(shard_part, up_w, preferred_element_type=jnp.float32)
    hidden = (jax.nn.silu(gate_part) * up_part).astype(jnp.bfloat16)
    partial_value = lax.optimization_barrier(
        jnp.dot(hidden, down_w, preferred_element_type=jnp.float32).astype(jnp.bfloat16)
    )
    summed = lax.psum_scatter(
        partial_value.astype(jnp.float32).astype(jnp.bfloat16),
        "tp",
        scatter_dimension=1,
        tiled=True,
    ).astype(jnp.float32)
    returned = lax.all_to_all(
        summed.astype(jnp.bfloat16), "ep", split_axis=0, concat_axis=0, tiled=True
    ).astype(summed.dtype)
    combined = jnp.sum(gate_weights[:, :, None] * returned[places], axis=1)
    squares_out = lax.psum(jnp.sum(combined * combined, axis=1), "tp")
    scale = lax.rsqrt(squares_out[:, None] / model_width + NORM_EPS)
    return (combined * scale * gain_out).astype(jnp.bfloat16)


def solution(mesh):
    placed = (
        P("ep", "tp"),
        P("ep", None),
        P("ep", None),
        P("tp"),
        P("tp"),
        P("ep", None, "tp"),
        P("ep", None, "tp"),
        P("ep", "tp", None),
    )
    return jax.shard_map(
        on_device, mesh=mesh, in_specs=placed, out_specs=P("ep", "tp"), check_vma=False
    )
```

profile of v0, /device:TPU:0, one launch (start us, length us, event | category | flops | bytes accessed | tf_op | source)
XLA Modules:
  0.0 177.8 jit_solution(11088431185920672371)
XLA Ops:
  6.5 0.0 all-gather.2.cloned.1.call-start
  6.5 0.8 copy.23
  7.3 0.1 eq.43
  7.5 0.1 eq.39
  7.6 0.6 reduce-window.6
  8.2 0.2 slice_reduce_fusion
  8.5 0.1 fusion.24
  8.6 0.1 reduce_sum.51
  8.7 0.1 copy.25
  8.8 0.7 compare_select_fusion
  9.5 0.1 fusion.20
  9.5 1.0 fusion.17
  10.6 11.4 %psum.14 = f32[128]{0:T(128)S(1)} all-reduce(f32[128]{0:T(128)S(1)} %fusion.17), channel_id=1, replica_groups=mesh['ep'=8,'tp'=4] {'tp'}, use_global_device_ids=true, to_apply=%region_5.6 | all-reduce | flops 128 | bytes 1024 | tf_op jit(solution)/shard_map/psum | solution.py:17
  22.0 1.3 convolution_convert_fusion
  23.2 20.1 %all_to_all.21 = bf16[8,64,512]{2,1,0:T(8,128)(2,1)} all-to-all(bf16[8,64,512]{2,1,0:T(8,128)(2,1)S(1)} %bitcast.33), channel_id=1, replica_groups=mesh['ep'=8,'tp'=4] {'ep'}, dimensions={0} | all-to-all | bytes 1048576 | tf_op jit(solution)/shard_map/all_to_all | solution.py:34
  43.3 0.0 all-gather.2.cloned.1.call-update
  43.4 0.0 reduce-scatter.2.cloned.1.call-start
  43.4 32.2 %all-gather.2.cloned.1.call-done = bf16[512,2048]{1,0:T(8,128)(2,1)} async-done(((bf16[512,512]{1,0:T(8,128)(2,1)}), bf16[512,2048]{1,0:T(8,128)(2,1)}) %all-gather.2.cloned.1.call-update) | async-done | bytes 2097168 | tf_op jit(solution)/shard_map/all_gather | solution.py:35
  75.6 0.0 copy-start.2
  75.6 10.6 %fusion.4 = f32[512,2048]{1,0:T(8,128)} fusion(bf16[512,2048]{1,0:T(8,128)(2,1)} %all-gather.2.cloned.1.call-done, bf16[1,2048,2048]{2,1,0:T(8,128)(2,1)} %param.13), kind=kOutput, calls=%fused_computation.5 | convolution fusion | flops 4294967296 | bytes 14680064 | tf_op jit(solution)/shard_map/dot_general | solution.py:36
  86.2 0.0 copy-done.2
  86.2 0.0 copy-start.1
  86.2 17.5 %fusion.10 = bf16[512,2048]{1,0:T(8,128)(2,1)} fusion(bf16[1,2048,2048]{2,1,0:T(8,128)(2,1)} %param.15, f32[512,2048]{1,0:T(8,128)} %fusion.4, bf16[512,2048]{1,0:T(8,128)(2,1)S(1)} %copy-done.2, bf16[1,2048,2048]{2,1,0:T(8,128)(2,1)} %param.14), kind=kOutput, calls=%fused_computation.8 | convolution fusion | flops 8597274624 | bytes 25165824 | tf_op jit(solution)/shard_map/dot_general | solution.py:40
  103.7 0.0 reduce-scatter.2.cloned.1.call-update
  103.7 35.3 %reduce-scatter.2.cloned.1.call-done = bf16[512,512]{1,0:T(8,128)(2,1)} async-done(((bf16[512,2048]{1,0:T(8,128)(2,1)}), bf16[512,512]{1,0:T(8,128)(2,1)}) %reduce-scatter.2.cloned.1.call-update) | async-done | bytes 524304 | tf_op jit(solution)/shard_map/reduce_scatter | solution.py:42
  139.0 4.6 %all-to-all-start.1 = ((bf16[8,64,512]{2,1,0:T(8,128)(2,1)}), bf16[8,64,512]{2,1,0:T(8,128)(2,1)S(1)}, u32[]{:S(2)}, u32[]{:S(2)}) async-start(bf16[8,64,512]{2,1,0:T(8,128)(2,1)} %bitcast.34), calls=%async_computation.2 | async-start | bytes 1048576 | tf_op jit(solution)/shard_map/all_to_all | solution.py:48
  143.6 0.1 copy.26
  143.8 0.1 reshape.49
  143.9 0.0 copy-done.1
  143.9 0.1 copy.22
  144.0 0.0 copy-start
  144.0 14.9 %all-to-all-done.1 = bf16[8,64,512]{2,1,0:T(8,128)(2,1)S(1)} async-done(((bf16[8,64,512]{2,1,0:T(8,128)(2,1)}), bf16[8,64,512]{2,1,0:T(8,128)(2,1)S(1)}, u32[]{:S(2)}, u32[]{:S(2)}) %all-to-all-start.1) | async-done | bytes 524320 | tf_op jit(solution)/shard_map/all_to_all | solution.py:48
  159.0 0.1 bitcast_convert_fusion
  159.1 1.0 gather_fusion
  160.1 0.3 reshape.48
  160.4 0.7 multiply_reduce_fusion
  161.1 0.1 multiply_reduce_fusion.1
  161.2 8.9 %psum.15 = f32[128]{0:T(128)S(1)} all-reduce(f32[128]{0:T(128)S(1)} %multiply_reduce_fusion.1), channel_id=1, replica_groups=mesh['ep'=8,'tp'=4] {'tp'}, use_global_device_ids=true, to_apply=%region_9.10 | all-reduce | flops 128 | bytes 1024 | tf_op jit(solution)/shard_map/psum | solution.py:52
  170.2 0.0 copy-done
  170.2 0.8 multiply_convert_fusion.1
  (6 shorter events, 0.1 us)
Async XLA Ops:
  6.5 69.1 %all-gather.2.cloned.1.call-start = ((), (), s32[]{:S(2)}) async-start(), calls=%async_computation.3 | async-start | bytes 2621440 | tf_op jit(solution)/shard_map/all_gather | solution.py:35
  43.4 95.7 %reduce-scatter.2.cloned.1.call-start = ((), (), s32[]{:S(2)}) async-start(), calls=%async_computation.4 | async-start | bytes 2621440 | tf_op jit(solution)/shard_map/reduce_scatter | solution.py:42
  75.6 10.6 %copy-start.2 = (bf16[512,2048]{1,0:T(8,128)(2,1)S(1)}, bf16[512,2048]{1,0:T(8,128)(2,1)}, u32[]{:S(2)}) copy-start(bf16[512,2048]{1,0:T(8,128)(2,1)} %all-gather.2.cloned.1.call-done) | copy-start | bytes 6291460
  86.2 57.7 %copy-start.1 = (f32[128,2]{0,1:T(2,128)S(1)}, f32[128,2]{0,1:T(2,128)}, u32[]{:S(2)}) copy-start(f32[128,2]{0,1:T(2,128)} %param.10) | copy-start | bytes 3076
  139.0 19.9 %all-to-all-start.1 = ((bf16[8,64,512]{2,1,0:T(8,128)(2,1)}), bf16[8,64,512]{2,1,0:T(8,128)(2,1)S(1)}, u32[]{:S(2)}, u32[]{:S(2)}) async-start(bf16[8,64,512]{2,1,0:T(8,128)(2,1)} %bitcast.34), calls=%async_computation.2 | async-start | bytes 1048576 | tf_op jit(solution)/shard_map/all_to_all | solution.py:48
  144.0 26.2 %copy-start = (f32[512]{0:T(512)S(1)}, f32[512]{0:T(512)}, u32[]{:S(2)}) copy-start(f32[512]{0:T(512)} %param.12) | copy-start | bytes 6148
Sparse Core Ops, SparseCore 0:
  43.5 32.0 all-gather.1
  103.8 35.1 reduce-scatter.1
where the time goes:
time: 178 us
  waiting for transfers between devices  82.5 us (46%)
  blocking collectives  40.4 us (23%)
  matrix products  29.3 us (16%)
  between operations  13.5 us (8%)
  starting transfers between devices  4.65 us (3%)
  other arithmetic  4.23 us (2%)
  local copies, waits for them, and re-layouts  3.14 us (2%)
    reduce_scatter x1, waiting for transfers between devices, on_device(): lax.psum_scatter(partial_value.astype(jnp.float32).astype(jnp.bfloat16),...  35.3 us
    all_gather x1, waiting for transfers between devices, on_device(): shard_part = lax.all_gather(arrived, 'tp', axis=1, tiled=True)  32.2 us
    all_to_all x1, blocking collectives, on_device(): lax.all_to_all(outgoing, 'ep', split_axis=0, concat_axis=0, tiled=True)  20.1 us
    dot_general x1, matrix products, on_device(): jnp.dot(hidden, down_w, preferred_element_type=jnp.float32)  17.5 us
    all_to_all x1, waiting for transfers between devices, on_device(): lax.all_to_all(summed.astype(jnp.bfloat16), 'ep', split_axis=0, concat_ax...  14.9 us
    psum x1, blocking collectives, on_device(): squares = lax.psum(jnp.sum(values * values, axis=1), 'tp')  11.4 us
    dot_general x1, matrix products, on_device(): gate_part = jnp.dot(shard_part, gate_w, preferred_element_type=jnp.float32)  10.6 us
    psum x1, blocking collectives, on_device(): squares_out = lax.psum(jnp.sum(combined * combined, axis=1), 'tp')  8.94 us
  transfers between devices with their start and end apart: 3, of which 3 were waited for; matrix products, arithmetic and copies ran while one was open for 0% of the time, Pallas kernels for 0%

commit v1 on v0

--- a/solution.py
+++ b/solution.py
@@ -49,7 +49,7 @@
         summed.astype(jnp.bfloat16), "ep", split_axis=0, concat_axis=0, tiled=True
     ).astype(summed.dtype)
     combined = jnp.sum(gate_weights[:, :, None] * returned[places], axis=1)
-    squares_out = lax.psum(jnp.sum(combined * combined, axis=1), "tp")
+    squares_out = jnp.sum(lax.all_gather(jnp.sum(combined * combined, axis=1), "tp"), axis=0)
     scale = lax.rsqrt(squares_out[:, None] / model_width + NORM_EPS)
     return (combined * scale * gain_out).astype(jnp.bfloat16)
 

time: 178 us -> 177 us (level)
    psum x1 -> x0, blocking collectives: 8.94 us -> none  [on_device(): squares_out = lax.psum(jnp.sum(combined * combined, axis=1), 'tp')]
    all_gather x0 -> x1, blocking collectives: none -> 7.91 us  [on_device(): lax.all_gather(jnp.sum(combined * combined, axis=1), 'tp')]
where the time goes in v1:
time: 177 us
  waiting for transfers between devices  82.5 us (47%)
  blocking collectives  39.4 us (22%)
  matrix products  29.3 us (17%)
  between operations  13.5 us (8%)
  starting transfers between devices  4.65 us (3%)
  other arithmetic  4.25 us (2%)
  local copies, waits for them, and re-layouts  3.14 us (2%)
    reduce_scatter x1, waiting for transfers between devices, on_device(): lax.psum_scatter(partial_value.astype(jnp.float32).astype(jnp.bfloat16),...  35.3 us
    all_gather x1, waiting for transfers between devices, on_device(): shard_part = lax.all_gather(arrived, 'tp', axis=1, tiled=True)  32.2 us
    all_to_all x1, blocking collectives, on_device(): lax.all_to_all(outgoing, 'ep', split_axis=0, concat_axis=0, tiled=True)  20.1 us
    dot_general x1, matrix products, on_device(): jnp.dot(hidden, down_w, preferred_element_type=jnp.float32)  17.5 us
    all_to_all x1, waiting for transfers between devices, on_device(): lax.all_to_all(summed.astype(jnp.bfloat16), 'ep', split_axis=0, concat_ax...  14.9 us
    psum x1, blocking collectives, on_device(): squares = lax.psum(jnp.sum(values * values, axis=1), 'tp')  11.4 us
    dot_general x1, matrix products, on_device(): gate_part = jnp.dot(shard_part, gate_w, preferred_element_type=jnp.float32)  10.6 us
    all_gather x1, blocking collectives, on_device(): lax.all_gather(jnp.sum(combined * combined, axis=1), 'tp')  7.91 us
  transfers between devices with their start and end apart: 3, of which 3 were waited for; matrix products, arithmetic and copies ran while one was open for 0% of the time, Pallas kernels for 0%

profile of v1, /device:TPU:0, one launch (start us, length us, event | category | flops | bytes accessed | tf_op | source)
XLA Modules:
  0.0 176.8 jit_solution(2650012142130354864)
XLA Ops:
  6.5 0.0 all-gather.4.cloned.1.call-start
  6.5 0.8 copy.28
  7.3 0.1 eq.43
  7.5 0.1 eq.39
  7.6 0.6 reduce-window.6
  8.2 0.2 slice_reduce_fusion
  8.5 0.1 fusion.24
  8.6 0.1 reduce_sum.60
  8.7 0.1 copy.30
  8.8 0.7 compare_select_fusion
  9.5 0.1 fusion.20
  9.5 1.0 fusion.17
  10.6 11.4 %psum.7 = f32[128]{0:T(128)S(1)} all-reduce(f32[128]{0:T(128)S(1)} %fusion.17), channel_id=1, replica_groups=mesh['ep'=8,'tp'=4] {'tp'}, use_global_device_ids=true, to_apply=%region_5.6 | all-reduce | flops 128 | bytes 1024 | tf_op jit(solution)/shard_map/psum | solution.py:17
  22.0 1.3 convolution_convert_fusion
  23.2 20.1 %all_to_all.21 = bf16[8,64,512]{2,1,0:T(8,128)(2,1)} all-to-all(bf16[8,64,512]{2,1,0:T(8,128)(2,1)S(1)} %bitcast.34), channel_id=1, replica_groups=mesh['ep'=8,'tp'=4] {'ep'}, dimensions={0} | all-to-all | bytes 1048576 | tf_op jit(solution)/shard_map/all_to_all | solution.py:34
  43.3 0.0 all-gather.4.cloned.1.call-update
  43.4 0.0 reduce-scatter.2.cloned.1.call-start
  43.4 32.2 %all-gather.4.cloned.1.call-done = bf16[512,2048]{1,0:T(8,128)(2,1)} async-done(((bf16[512,512]{1,0:T(8,128)(2,1)}), bf16[512,2048]{1,0:T(8,128)(2,1)}) %all-gather.4.cloned.1.call-update) | async-done | bytes 2097168 | tf_op jit(solution)/shard_map/all_gather | solution.py:35
  75.6 0.0 copy-start.2
  75.6 10.6 %fusion.4 = f32[512,2048]{1,0:T(8,128)} fusion(bf16[512,2048]{1,0:T(8,128)(2,1)} %all-gather.4.cloned.1.call-done, bf16[1,2048,2048]{2,1,0:T(8,128)(2,1)} %param.13), kind=kOutput, calls=%fused_computation.5 | convolution fusion | flops 4294967296 | bytes 14680064 | tf_op jit(solution)/shard_map/dot_general | solution.py:36
  86.2 0.0 copy-done.2
  86.2 0.0 copy-start.1
  86.2 17.5 %fusion.10 = bf16[512,2048]{1,0:T(8,128)(2,1)} fusion(bf16[1,2048,2048]{2,1,0:T(8,128)(2,1)} %param.15, f32[512,2048]{1,0:T(8,128)} %fusion.4, bf16[512,2048]{1,0:T(8,128)(2,1)S(1)} %copy-done.2, bf16[1,2048,2048]{2,1,0:T(8,128)(2,1)} %param.14), kind=kOutput, calls=%fused_computation.8 | convolution fusion | flops 8597274624 | bytes 25165824 | tf_op jit(solution)/shard_map/dot_general | solution.py:40
  103.7 0.0 reduce-scatter.2.cloned.1.call-update
  103.7 35.3 %reduce-scatter.2.cloned.1.call-done = bf16[512,512]{1,0:T(8,128)(2,1)} async-done(((bf16[512,2048]{1,0:T(8,128)(2,1)}), bf16[512,512]{1,0:T(8,128)(2,1)}) %reduce-scatter.2.cloned.1.call-update) | async-done | bytes 524304 | tf_op jit(solution)/shard_map/reduce_scatter | solution.py:42
  139.0 4.6 %all-to-all-start.1 = ((bf16[8,64,512]{2,1,0:T(8,128)(2,1)}), bf16[8,64,512]{2,1,0:T(8,128)(2,1)S(1)}, u32[]{:S(2)}, u32[]{:S(2)}) async-start(bf16[8,64,512]{2,1,0:T(8,128)(2,1)} %bitcast.35), calls=%async_computation.2 | async-start | bytes 1048576 | tf_op jit(solution)/shard_map/all_to_all | solution.py:48
  143.6 0.1 copy.31
  143.8 0.1 reshape.53
  143.9 0.0 copy-done.1
  143.9 0.1 copy.27
  144.0 0.0 copy-start
  144.0 14.9 %all-to-all-done.1 = bf16[8,64,512]{2,1,0:T(8,128)(2,1)S(1)} async-done(((bf16[8,64,512]{2,1,0:T(8,128)(2,1)}), bf16[8,64,512]{2,1,0:T(8,128)(2,1)S(1)}, u32[]{:S(2)}, u32[]{:S(2)}) %all-to-all-start.1) | async-done | bytes 524320 | tf_op jit(solution)/shard_map/all_to_all | solution.py:48
  159.0 0.1 bitcast_convert_fusion
  159.1 1.0 gather_fusion
  160.1 0.3 reshape.52
  160.4 0.7 multiply_reduce_fusion
  161.1 0.1 multiply_reduce_fusion.1
  161.2 7.9 %all-gather.1 = f32[4,1,128]{2,1,0:T(1,128)S(1)} all-gather(f32[1,1,128]{2,1,0:T(1,128)S(1)} %bitcast.36), channel_id=2, replica_groups=mesh['ep'=8,'tp'=4] {'tp'}, dimensions={0}, use_global_device_ids=true | all-gather | bytes 2560 | tf_op jit(solution)/shard_map/all_gather | solution.py:52
  169.2 0.0 copy-done
  169.2 0.8 multiply_convert_fusion.1
  (7 shorter events, 0.1 us)
Async XLA Ops:
  6.5 69.1 %all-gather.4.cloned.1.call-start = ((), (), s32[]{:S(2)}) async-start(), calls=%async_computation.3 | async-start | bytes 2621440 | tf_op jit(solution)/shard_map/all_gather | solution.py:35
  43.4 95.7 %reduce-scatter.2.cloned.1.call-start = ((), (), s32[]{:S(2)}) async-start(), calls=%async_computation.4 | async-start | bytes 2621440 | tf_op jit(solution)/shard_map/reduce_scatter | solution.py:42
  75.6 10.6 %copy-start.2 = (bf16[512,2048]{1,0:T(8,128)(2,1)S(1)}, bf16[512,2048]{1,0:T(8,128)(2,1)}, u32[]{:S(2)}) copy-start(bf16[512,2048]{1,0:T(8,128)(2,1)} %all-gather.4.cloned.1.call-done) | copy-start | bytes 6291460
  86.2 57.7 %copy-start.1 = (f32[128,2]{0,1:T(2,128)S(1)}, f32[128,2]{0,1:T(2,128)}, u32[]{:S(2)}) copy-start(f32[128,2]{0,1:T(2,128)} %param.10) | copy-start | bytes 3076
  139.0 19.9 %all-to-all-start.1 = ((bf16[8,64,512]{2,1,0:T(8,128)(2,1)}), bf16[8,64,512]{2,1,0:T(8,128)(2,1)S(1)}, u32[]{:S(2)}, u32[]{:S(2)}) async-start(bf16[8,64,512]{2,1,0:T(8,128)(2,1)} %bitcast.35), calls=%async_computation.2 | async-start | bytes 1048576 | tf_op jit(solution)/shard_map/all_to_all | solution.py:48
  144.0 25.1 %copy-start = (f32[512]{0:T(512)S(1)}, f32[512]{0:T(512)}, u32[]{:S(2)}) copy-start(f32[512]{0:T(512)} %param.12) | copy-start | bytes 6148
Sparse Core Ops, SparseCore 0:
  43.5 32.0 all-gather.3
  103.8 35.1 reduce-scatter.1

commit v2 on v0

--- a/solution.py
+++ b/solution.py
@@ -32,7 +32,7 @@
     down_w = w_down[0]
     outgoing = jnp.dot(picker, normed, preferred_element_type=jnp.float32).astype(jnp.bfloat16)
     arrived = lax.all_to_all(outgoing, "ep", split_axis=0, concat_axis=0, tiled=True)
-    shard_part = lax.all_gather(arrived, "tp", axis=1, tiled=True)
+    shard_part = jnp.concatenate(lax.all_gather(arrived, "tp"), axis=1)
     gate_part = jnp.dot(shard_part, gate_w, preferred_element_type=jnp.float32)
     up_part = jnp.dot(shard_part, up_w, preferred_element_type=jnp.float32)
     hidden = (jax.nn.silu(gate_part) * up_part).astype(jnp.bfloat16)

time: 178 us -> 181 us (1.017)
  local copies, waits for them, and re-layouts: 3.14 us -> 5.92 us
    all_gather x0 -> x1, local copies, waits for them, and re-layouts: none -> 2.79 us  [on_device(): shard_part = jnp.concatenate(lax.all_gather(arrived, 'tp'), axis=1)]
where the time goes in v2:
time: 181 us; the launch traced here: 180 us
  waiting for transfers between devices  82.6 us (46%)
  blocking collectives  40.4 us (22%)
  matrix products  28.7 us (16%)
  between operations  13.5 us (7%)
  local copies, waits for them, and re-layouts  5.92 us (3%)
  starting transfers between devices  4.65 us (3%)
  other arithmetic  4.23 us (2%)
    reduce_scatter x1, waiting for transfers between devices, on_device(): lax.psum_scatter(partial_value.astype(jnp.float32).astype(jnp.bfloat16),...  35.3 us
    all_gather x1, waiting for transfers between devices, on_device(): shard_part = jnp.concatenate(lax.all_gather(arrived, 'tp'), axis=1)  32.3 us
    all_to_all x1, blocking collectives, on_device(): lax.all_to_all(outgoing, 'ep', split_axis=0, concat_axis=0, tiled=True)  20.1 us
    dot_general x1, matrix products, on_device(): jnp.dot(hidden, down_w, preferred_element_type=jnp.float32)  18 us
    all_to_all x1, waiting for transfers between devices, on_device(): lax.all_to_all(summed.astype(jnp.bfloat16), 'ep', split_axis=0, concat_ax...  14.9 us
    psum x1, blocking collectives, on_device(): squares = lax.psum(jnp.sum(values * values, axis=1), 'tp')  11.4 us
    dot_general x1, matrix products, on_device(): gate_part = jnp.dot(shard_part, gate_w, preferred_element_type=jnp.float32)  9.43 us
    psum x1, blocking collectives, on_device(): squares_out = lax.psum(jnp.sum(combined * combined, axis=1), 'tp')  8.94 us
  transfers between devices with their start and end apart: 3, of which 3 were waited for; matrix products, arithmetic and copies ran while one was open for 0% of the time, Pallas kernels for 0%

profile of v2, /device:TPU:0, one launch (start us, length us, event | category | flops | bytes accessed | tf_op | source)
XLA Modules:
  0.0 180.1 jit_solution(5731504696938454310)
XLA Ops:
  6.5 0.0 all-gather.2.cloned.1.call-start
  6.5 0.8 copy.37
  7.3 0.1 eq.43
  7.5 0.1 eq.39
  7.6 0.6 reduce-window.6
  8.2 0.2 slice_reduce_fusion
  8.5 0.1 fusion.24
  8.6 0.1 reduce_sum.51
  8.7 0.1 copy.39
  8.8 0.7 compare_select_fusion
  9.5 0.1 fusion.20
  9.5 1.0 fusion.17
  10.6 11.4 %psum.14 = f32[128]{0:T(128)S(1)} all-reduce(f32[128]{0:T(128)S(1)} %fusion.17), channel_id=1, replica_groups=mesh['ep'=8,'tp'=4] {'tp'}, use_global_device_ids=true, to_apply=%region_5.6 | all-reduce | flops 128 | bytes 1024 | tf_op jit(solution)/shard_map/psum | solution.py:17
  22.0 1.3 convolution_convert_fusion
  23.2 20.1 %all_to_all.18 = bf16[8,64,512]{2,1,0:T(8,128)(2,1)} all-to-all(bf16[8,64,512]{2,1,0:T(8,128)(2,1)S(1)} %bitcast.38), channel_id=1, replica_groups=mesh['ep'=8,'tp'=4] {'ep'}, dimensions={0} | all-to-all | bytes 1048576 | tf_op jit(solution)/shard_map/all_to_all | solution.py:34
  43.3 0.0 all-gather.2.cloned.1.call-update
  43.4 0.0 reduce-scatter.2.cloned.1.call-start
  43.4 32.3 %all-gather.2.cloned.1.call-done = bf16[4,512,512]{2,1,0:T(8,128)(2,1)} async-done(((bf16[1,512,512]{2,1,0:T(8,128)(2,1)}), bf16[4,512,512]{2,1,0:T(8,128)(2,1)}) %all-gather.2.cloned.1.call-update) | async-done | bytes 2097168 | tf_op jit(solution)/shard_map/all_gather | solution.py:35
  75.8 2.8 %copy.40 = bf16[4,512,512]{1,2,0:T(8,128)(2,1)S(1)} copy(bf16[4,512,512]{2,1,0:T(8,128)(2,1)} %all-gather.2.cloned.1.call-done) | data formatting | bytes 4194304 | tf_op jit(solution)/shard_map/all_gather | solution.py:35
  78.5 9.4 %fusion.4 = f32[512,2048]{1,0:T(8,128)} fusion(bf16[512,2048]{0,1:T(8,128)(2,1)S(1)} %bitcast.35, bf16[1,2048,2048]{2,1,0:T(8,128)(2,1)} %param.13), kind=kOutput, calls=%fused_computation.5 | convolution fusion | flops 4294967296 | bytes 14680064 | tf_op jit(solution)/shard_map/dot_general | solution.py:36
  88.0 0.0 copy-start.1
  88.0 18.0 %fusion.10 = bf16[512,2048]{1,0:T(8,128)(2,1)} fusion(bf16[1,2048,2048]{2,1,0:T(8,128)(2,1)} %param.15, f32[512,2048]{1,0:T(8,128)} %fusion.4, bf16[512,2048]{0,1:T(8,128)(2,1)S(1)} %bitcast.36, bf16[1,2048,2048]{2,1,0:T(8,128)(2,1)} %param.14), kind=kOutput, calls=%fused_computation.8 | convolution fusion | flops 8597274624 | bytes 25165824 | tf_op jit(solution)/shard_map/dot_general | solution.py:40
  106.0 0.0 reduce-scatter.2.cloned.1.call-update
  106.0 35.3 %reduce-scatter.2.cloned.1.call-done = bf16[512,512]{1,0:T(8,128)(2,1)} async-done(((bf16[512,2048]{1,0:T(8,128)(2,1)}), bf16[512,512]{1,0:T(8,128)(2,1)}) %reduce-scatter.2.cloned.1.call-update) | async-done | bytes 524304 | tf_op jit(solution)/shard_map/reduce_scatter | solution.py:42
  141.4 4.6 %all-to-all-start.1 = ((bf16[8,64,512]{2,1,0:T(8,128)(2,1)}), bf16[8,64,512]{2,1,0:T(8,128)(2,1)S(1)}, u32[]{:S(2)}, u32[]{:S(2)}) async-start(bf16[8,64,512]{2,1,0:T(8,128)(2,1)} %bitcast.39), calls=%async_computation.2 | async-start | bytes 1048576 | tf_op jit(solution)/shard_map/all_to_all | solution.py:48
  146.0 0.1 copy.41
  146.1 0.1 reshape.58
  146.2 0.0 copy-done.1
  146.2 0.1 copy.36
  146.3 0.0 copy-start
  146.3 14.9 %all-to-all-done.1 = bf16[8,64,512]{2,1,0:T(8,128)(2,1)S(1)} async-done(((bf16[8,64,512]{2,1,0:T(8,128)(2,1)}), bf16[8,64,512]{2,1,0:T(8,128)(2,1)S(1)}, u32[]{:S(2)}, u32[]{:S(2)}) %all-to-all-start.1) | async-done | bytes 524320 | tf_op jit(solution)/shard_map/all_to_all | solution.py:48
  161.3 0.1 bitcast_convert_fusion
  161.4 1.0 gather_fusion
  162.4 0.3 reshape.57
  162.7 0.7 multiply_reduce_fusion
  163.4 0.1 multiply_reduce_fusion.1
  163.5 8.9 %psum.15 = f32[128]{0:T(128)S(1)} all-reduce(f32[128]{0:T(128)S(1)} %multiply_reduce_fusion.1), channel_id=1, replica_groups=mesh['ep'=8,'tp'=4] {'tp'}, use_global_device_ids=true, to_apply=%region_9.10 | all-reduce | flops 128 | bytes 1024 | tf_op jit(solution)/shard_map/psum | solution.py:52
  172.5 0.0 copy-done
  172.5 0.8 multiply_convert_fusion.1
  (6 shorter events, 0.1 us)
Async XLA Ops:
  6.5 69.2 %all-gather.2.cloned.1.call-start = ((), (), s32[]{:S(2)}) async-start(), calls=%async_computation.3 | async-start | bytes 2621440 | tf_op jit(solution)/shard_map/all_gather | solution.py:35
  43.4 98.0 %reduce-scatter.2.cloned.1.call-start = ((), (), s32[]{:S(2)}) async-start(), calls=%async_computation.4 | async-start | bytes 2621440 | tf_op jit(solution)/shard_map/reduce_scatter | solution.py:42
  88.0 58.2 %copy-start.1 = (f32[128,2]{0,1:T(2,128)S(1)}, f32[128,2]{0,1:T(2,128)}, u32[]{:S(2)}) copy-start(f32[128,2]{0,1:T(2,128)} %param.10) | copy-start | bytes 3076
  141.4 19.9 %all-to-all-start.1 = ((bf16[8,64,512]{2,1,0:T(8,128)(2,1)}), bf16[8,64,512]{2,1,0:T(8,128)(2,1)S(1)}, u32[]{:S(2)}, u32[]{:S(2)}) async-start(bf16[8,64,512]{2,1,0:T(8,128)(2,1)} %bitcast.39), calls=%async_computation.2 | async-start | bytes 1048576 | tf_op jit(solution)/shard_map/all_to_all | solution.py:48
  146.3 26.2 %copy-start = (f32[512]{0:T(512)S(1)}, f32[512]{0:T(512)}, u32[]{:S(2)}) copy-start(f32[512]{0:T(512)} %param.12) | copy-start | bytes 6148
Sparse Core Ops, SparseCore 0:
  43.5 32.2 all-gather.1
  106.1 35.1 reduce-scatter.1
